TPU v7x, 512 devices: a whole 4x4x16 slice. The times are simulated.
512 devices in a mesh: ep: 32 (over z, core), tp: 16 (over y, x).
Axes of the slice: x: 4, y: 4, z: 16, core: 2. Of those that a mesh axis runs over, the one named last changes fastest.
Arguments:
- tokens: bfloat16 [8192, 2048], P('ep', 'tp'), may hold values from -800 to 800
- norm_gain: bfloat16 [2048], P('tp'), may hold values from 0.099609375 to 1.8984375
- w_gate: bfloat16 [32, 2048, 6144], P('ep', None, 'tp'), may hold values from -0.125 to 0.125
- w_up: bfloat16 [32, 2048, 6144], P('ep', None, 'tp'), may hold values from -0.125 to 0.125
- w_down: bfloat16 [32, 6144, 2048], P('ep', 'tp'), may hold values from -1.2757759 to 1.2757759
- routes: int32 [8192, 2], P('ep'), may hold values from 0 to 31, all different within a row; in each aligned block of 256 rows (0 to 255, 256 to 511, ...) at most 32 rows name the same one
- route_weights: float32 [8192, 2], P('ep'), may hold values from 0.1 to 1
- final_gain: bfloat16 [2048], P('tp'), may hold values from 0.099609375 to 1.8984375
Outputs:
- mixed_out: bfloat16 [8192, 2048], P('ep', 'tp')
Inputs may be any that keep to these rules, and one draw needn't show every extreme that they name: `routes`: A token's 2 experts differ. Among the tokens of one index of ep (aligned blocks of 256 rows), no expert is named by more than 32 tokens, a bound that some block reaches.
All inputs are finite; a program needn't handle non-finite values.
Results may differ from a plain program's by a relative error of at most 0.017.
Values may be sent and summed in bfloat16 or wider, within the bound.
A program may use at most 64 MiB of HBM per device.

v0:
```python
import jax
import jax.numpy as jnp
from jax import lax
from jax.sharding import PartitionSpec as P

EPS = 1e-06


def from_everyone(shard, axis):
    copies = jnp.broadcast_to(shard, (lax.axis_size(axis), *shard.shape))
    return lax.all_to_all(copies, axis, split_axis=0, concat_axis=0, tiled=True)


def over_copies(shard, axis):
    return from_everyone(shard, axis).sum(axis=0)


def cut_along(shard, dim, length):
    before, after = (shard.shape[:dim], shard.shape[dim + 1 :])
    return jnp.moveaxis(shard.reshape(*before, length, -1, *after), dim, 0)


def summed_on_arrival(shard, axis, dim):
    length = lax.axis_size(axis)
    tiles = lax.all_to_all(cut_along(shard, dim, length), axis, 0, 0, tiled=True)
    return jnp.sum(tiles.astype(jnp.float32), axis=0)


def slot_targets(routes, experts, capacity):
    flat = routes.reshape(-1)
    onehot = (flat[:, None] == jnp.arange(experts, dtype=jnp.int32)[None, :]).astype(jnp.int32)
    before = jnp.cumsum(onehot, axis=0) - onehot
    slot = jnp.sum(before * onehot, axis=1)
    return flat * capacity + slot


def local(tokens, norm_gain, w_gate, w_up, w_down, routes, route_weights, final_gain):
    experts = lax.axis_size("ep")
    tok_rows = tokens.shape[0]
    share = tokens.shape[1]
    width = share * lax.axis_size("tp")
    topk = routes.shape[1]
    capacity = 2 * tok_rows * topk // experts
    wide = tokens.astype(jnp.float32)
    input_squares = over_copies(jnp.sum(wide * wide, axis=1), "tp")
    scale = lax.rsqrt(input_squares / width + EPS)
    normed = (wide * scale[:, None] * norm_gain.astype(jnp.float32)[None, :]).astype(jnp.bfloat16)
    target = slot_targets(routes, experts, capacity)
    sources = jnp.repeat(jnp.arange(tok_rows, dtype=jnp.int32), topk)
    gate_w = w_gate[0]
    up_w = w_up[0]
    down_w = w_down[0]
    outbox = jnp.zeros((experts * capacity, share), jnp.bfloat16).at[target].set(normed[sources])
    inbox = lax.all_to_all(outbox, "ep", split_axis=0, concat_axis=0, tiled=True)
    piece = lax.all_gather(inbox, "tp", axis=1, tiled=True)
    gate = jnp.dot(piece, gate_w, preferred_element_type=jnp.float32)
    up = jnp.dot(piece, up_w, preferred_element_type=jnp.float32)
    hidden = (jax.nn.silu(gate) * up).astype(jnp.bfloat16)
    sums = summed_on_arrival(
        lax.dot_general(
            down_w, hidden, (((0,), (1,)), ((), ())), preferred_element_type=jnp.float32
        ).astype(jnp.bfloat16),
        "tp",
        0,
    )
    returned = lax.all_to_all(
        sums.astype(jnp.bfloat16), "ep", split_axis=1, concat_axis=1, tiled=True
    )
    picked = jnp.take(returned, target, axis=1).reshape(returned.shape[0], tok_rows, topk)
    combined = jnp.einsum("dtk,tk->td", picked.astype(jnp.float32), route_weights)
    local_squares = jnp.sum(combined * combined, axis=1)
    total_squares = over_copies(local_squares, "tp")
    final_scale = lax.rsqrt(total_squares / width + EPS)
    return (combined * final_scale[:, None] * final_gain.astype(jnp.float32)[None, :]).astype(
        jnp.bfloat16
    )


def solution(mesh):
    in_specs = (
        P("ep", "tp"),
        P("tp"),
        P("ep", None, "tp"),
        P("ep", None, "tp"),
        P("ep", "tp", None),
        P("ep", None),
        P("ep", None),
        P("tp"),
    )
    out_specs = P("ep", "tp")
    return jax.shard_map(local, mesh=mesh, in_specs=in_specs, out_specs=out_specs, check_vma=False)
```

profile of v0, /device:TPU:1, one launch (start us, length us, event | category | flops | bytes accessed | tf_op | source)
XLA Modules:
  0.0 259.8 jit_solution(18186526171175588482)
XLA Ops:
  6.5 0.0 copy-start
  6.5 0.0 copy-start.3
  6.5 1.1 fusion.9
  7.6 0.6 broadcast_in_dim.31
  8.3 7.6 %all-to-all-start = ((f32[16,1,256]{2,1,0:T(1,128)}), f32[16,1,256]{2,1,0:T(1,128)S(1)}, u32[]{:S(2)}, u32[]{:S(2)}) async-start(f32[16,1,256]{2,1,0:T(1,128)} %broadcast_in_dim.31), calls=%async_computation | async-start | bytes 32768 | tf_op jit(solution)/shard_map/all_to_all | solution.py:11
  15.8 0.0 all-gather.2.cloned.1.call-start
  15.9 0.8 copy.31
  16.7 0.1 eq.26
  16.9 0.1 reshape.120
  17.0 0.7 broadcast_multiply_fusion
  17.7 1.2 reduce-window.6
  18.9 0.2 slice_reduce_fusion
  19.1 0.1 copy.36
  19.3 0.1 mul.70
  19.4 0.1 reshape.122
  19.6 0.1 fusion.18
  19.7 0.7 convert_element_type.37
  20.4 1.9 all-to-all-done
  22.3 0.9 fusion.11
  23.3 3.1 %scatter_custom_fusion = bf16[1024,128]{1,0:T(8,128)(2,1)S(1)} fusion(s32[512]{0:T(512)S(1)} %bitcast.62, bf16[256,128]{1,0:T(8,128)(2,1)S(1)} %fusion.11, s32[1024]{0:T(1024)S(1)} %pad_clamp_fusion.1, bf16[]{:T(256)} %constant.34.clone.1), kind=kCustom, calls=%fused_computation.17 | custom fusion | bytes 262146 | tf_op jit(solution)/shard_map/scatter | solution.py:53
  26.3 39.5 %all_to_all.41 = bf16[32,32,128]{2,1,0:T(8,128)(2,1)} all-to-all(bf16[32,32,128]{2,1,0:T(8,128)(2,1)S(1)} %bitcast.57), channel_id=1, replica_groups=mesh['ep'=32,'tp'=16] {'ep'}, dimensions={0} | all-to-all | bytes 524288 | tf_op jit(solution)/shard_map/all_to_all | solution.py:54
  65.9 0.0 all-gather.2.cloned.1.call-update
  65.9 59.4 %all-gather.2.cloned.1.call-done = bf16[1024,2048]{1,0:T(8,128)(2,1)} async-done(((bf16[1024,128]{1,0:T(8,128)(2,1)}), bf16[1024,2048]{1,0:T(8,128)(2,1)}) %all-gather.2.cloned.1.call-update) | async-done | bytes 4194320 | tf_op jit(solution)/shard_map/all_gather | solution.py:55
  125.3 0.0 copy-done.3
  125.3 5.7 %fusion.3 = f32[1024,384]{1,0:T(8,128)} fusion(bf16[1024,2048]{1,0:T(8,128)(2,1)} %all-gather.2.cloned.1.call-done, bf16[1,2048,384]{2,1,0:T(8,128)(2,1)S(1)} %copy-done.3), kind=kOutput, calls=%fused_computation.8 | convolution fusion | flops 1610612736 | bytes 7340032 | tf_op jit(solution)/shard_map/dot_general | solution.py:56
  131.0 0.0 copy-done
  131.0 9.6 %convert_bitcast_fusion = bf16[128,16,8,128]{3,2,1,0:T(8,128)(2,1)} fusion(bf16[1,384,2048]{2,1,0:T(8,128)(2,1)S(1)} %copy-done, f32[1024,384]{1,0:T(8,128)} %fusion.3, bf16[1024,2048]{1,0:T(8,128)(2,1)} %all-gather.2.cloned.1.call-done, bf16[1,2048,384]{2,1,0:T(8,128)(2,1)} %param.11), kind=kOutput, calls=%fused_computation.4 | convolution fusion | flops 3225681920 | bytes 13107200 | tf_op jit(solution)/shard_map/dot_general | solution.py:60
  140.6 3.3 %copy.48 = bf16[128,16,8,128]{3,2,0,1:T(8,128)(2,1)S(1)} copy(bf16[128,16,8,128]{3,2,1,0:T(8,128)(2,1)} %convert_bitcast_fusion) | data formatting | bytes 8388608 | tf_op jit(solution)/shard_map/reshape | solution.py:20
  143.9 54.5 %all_to_all.42 = bf16[16,128,1024]{1,2,0:T(8,128)(2,1)} all-to-all(bf16[16,128,1024]{1,2,0:T(8,128)(2,1)S(1)} %bitcast.54), channel_id=1, replica_groups=mesh['ep'=32,'tp'=16] {'tp'}, dimensions={0} | all-to-all | bytes 8388608 | tf_op jit(solution)/shard_map/all_to_all | solution.py:25
  198.3 0.0 copy-start.1
  198.3 0.0 copy-start.2
  198.3 3.5 %reduce_sum.66 = bf16[128,1024]{0,1:T(8,128)(2,1)} reduce(bf16[16,128,1024]{1,2,0:T(8,128)(2,1)} %all_to_all.42, bf16[]{:T(256)} %constant.34.clone.1), dimensions={0}, to_apply=%region_6.7 | reduce | flops 1966080 | bytes 4456450 | tf_op jit(solution)/shard_map/reduce_sum | solution.py:26
  201.9 15.5 %all-to-all-start.3 = ((bf16[128,32,32]{0,2,1:T(8,128)(2,1)}), bf16[128,32,32]{0,2,1:T(8,128)(2,1)S(1)}, u32[]{:S(2)}, u32[]{:S(2)}) async-start(bf16[128,32,32]{0,2,1:T(8,128)(2,1)} %bitcast.10), calls=%async_computation.3 | async-start | bytes 524288 | tf_op jit(solution)/shard_map/all_to_all | solution.py:66
  217.4 0.1 reduce_sum.62
  217.5 0.1 copy.34
  217.6 0.0 copy-done.1
  217.6 0.2 copy.35
  217.8 0.0 copy-done.2
  217.8 0.2 copy.40
  218.0 21.6 %all-to-all-done.3 = bf16[128,32,32]{0,2,1:T(8,128)(2,1)S(1)} async-done(((bf16[128,32,32]{0,2,1:T(8,128)(2,1)}), bf16[128,32,32]{0,2,1:T(8,128)(2,1)S(1)}, u32[]{:S(2)}, u32[]{:S(2)}) %all-to-all-start.3) | async-done | bytes 262176 | tf_op jit(solution)/shard_map/all_to_all | solution.py:66
  239.7 0.0 copy-start.4
  239.7 1.3 gather_fusion
  241.0 0.5 fusion.15
  241.5 0.1 multiply_reduce_fusion
  241.6 0.6 broadcast_in_dim.34
  242.2 3.5 %all-to-all-start.4 = ((f32[16,1,256]{2,1,0:T(1,128)}), f32[16,1,256]{2,1,0:T(1,128)S(1)}, u32[]{:S(2)}, u32[]{:S(2)}) async-start(f32[16,1,256]{2,1,0:T(1,128)} %broadcast_in_dim.34), calls=%async_computation.4 | async-start | bytes 32768 | tf_op jit(solution)/shard_map/all_to_all | solution.py:11
  245.8 0.0 copy-done.4
  245.8 6.4 %all-to-all-done.4 = f32[16,1,256]{2,1,0:T(1,128)S(1)} async-done(((f32[16,1,256]{2,1,0:T(1,128)}), f32[16,1,256]{2,1,0:T(1,128)S(1)}, u32[]{:S(2)}, u32[]{:S(2)}) %all-to-all-start.4) | async-done | bytes 16416 | tf_op jit(solution)/shard_map/all_to_all | solution.py:11
  252.2 0.7 multiply_convert_fusion.1
  (14 shorter events, 0.2 us)
Async XLA Ops:
  6.5 124.5 %copy-start = (bf16[1,384,2048]{2,1,0:T(8,128)(2,1)S(1)}, bf16[1,384,2048]{2,1,0:T(8,128)(2,1)}, u32[]{:S(2)}) copy-start(bf16[1,384,2048]{2,1,0:T(8,128)(2,1)} %param.12) | copy-start | bytes 4718596
  6.5 118.7 %copy-start.3 = (bf16[1,2048,384]{2,1,0:T(8,128)(2,1)S(1)}, bf16[1,2048,384]{2,1,0:T(8,128)(2,1)}, u32[]{:S(2)}) copy-start(bf16[1,2048,384]{2,1,0:T(8,128)(2,1)} %param.10) | copy-start | bytes 4718596
  8.3 14.0 %all-to-all-start = ((f32[16,1,256]{2,1,0:T(1,128)}), f32[16,1,256]{2,1,0:T(1,128)S(1)}, u32[]{:S(2)}, u32[]{:S(2)}) async-start(f32[16,1,256]{2,1,0:T(1,128)} %broadcast_in_dim.31), calls=%async_computation | async-start | bytes 32768 | tf_op jit(solution)/shard_map/all_to_all | solution.py:11
  15.8 109.4 %all-gather.2.cloned.1.call-start = ((), (), s32[]{:S(2)}) async-start(), calls=%async_computation.5 | async-start | bytes 4456448 | tf_op jit(solution)/shard_map/all_gather | solution.py:55
  198.3 19.3 %copy-start.1 = (s32[256,2]{0,1:T(2,128)S(1)}, s32[256,2]{0,1:T(2,128)}, u32[]{:S(2)}) copy-start(s32[256,2]{0,1:T(2,128)} %param.13) | copy-start | bytes 6148
  198.3 19.5 %copy-start.2 = (f32[256,2]{0,1:T(2,128)S(1)}, f32[256,2]{0,1:T(2,128)}, u32[]{:S(2)}) copy-start(f32[256,2]{0,1:T(2,128)} %param.14) | copy-start | bytes 6148
  201.9 37.8 %all-to-all-start.3 = ((bf16[128,32,32]{0,2,1:T(8,128)(2,1)}), bf16[128,32,32]{0,2,1:T(8,128)(2,1)S(1)}, u32[]{:S(2)}, u32[]{:S(2)}) async-start(bf16[128,32,32]{0,2,1:T(8,128)(2,1)} %bitcast.10), calls=%async_computation.3 | async-start | bytes 524288 | tf_op jit(solution)/shard_map/all_to_all | solution.py:66
  239.7 6.1 %copy-start.4 = (bf16[128]{0:T(256)(128)(2,1)S(1)}, bf16[128]{0:T(256)(128)(2,1)}, u32[]{:S(2)}) copy-start(bf16[128]{0:T(256)(128)(2,1)} %param.15) | copy-start | bytes 772
  242.2 9.9 %all-to-all-start.4 = ((f32[16,1,256]{2,1,0:T(1,128)}), f32[16,1,256]{2,1,0:T(1,128)S(1)}, u32[]{:S(2)}, u32[]{:S(2)}) async-start(f32[16,1,256]{2,1,0:T(1,128)} %broadcast_in_dim.34), calls=%async_computation.4 | async-start | bytes 32768 | tf_op jit(solution)/shard_map/all_to_all | solution.py:11
Sparse Core Ops, SparseCore 0:
  66.0 59.2 all-gather.1
where the time goes:
time: 260 us
  blocking collectives  94 us (36%)
  waiting for transfers between devices  89.3 us (34%)
  starting transfers between devices  26.6 us (10%)
  matrix products  15.8 us (6%)
  between operations  13.6 us (5%)
  local copies, waits for them, and re-layouts  11.2 us (4%)
  other arithmetic  9.22 us (4%)
    all_gather x1, waiting for transfers between devices, local(): piece = lax.all_gather(inbox, 'tp', axis=1, tiled=True)  59.4 us
    all_to_all x1, blocking collectives, summed_on_arrival(): lax.all_to_all(cut_along(shard, dim, length), axis, 0, 0, tiled=True)  54.5 us
    all_to_all x1, blocking collectives, local(): lax.all_to_all(outbox, 'ep', split_axis=0, concat_axis=0, tiled=True)  39.5 us
    all_to_all x1, waiting for transfers between devices, local(): lax.all_to_all(sums.astype(jnp.bfloat16), 'ep', split_axis=1, concat_axis...  21.6 us
    all_to_all x1, starting transfers between devices, local(): lax.all_to_all(sums.astype(jnp.bfloat16), 'ep', split_axis=1, concat_axis...  15.5 us
    all_to_all x2, starting transfers between devices, from_everyone(): return lax.all_to_all(copies, axis, split_axis=0, concat_axis=0, tiled=True)  11.1 us
    dot_general x1, matrix products, local(): lax.dot_general(down_w, hidden, (((0,), (1,)), ((), ())), preferred_eleme...  9.6 us
    all_to_all x2, waiting for transfers between devices, from_everyone(): return lax.all_to_all(copies, axis, split_axis=0, concat_axis=0, tiled=True)  8.25 us
  transfers between devices with their start and end apart: 4, of which 4 were waited for; matrix products, arithmetic and copies ran while one was open for 2% of the time, Pallas kernels for 0%

commit v1 on v0

--- a/solution.py
+++ b/solution.py
@@ -4,6 +4,12 @@
 from jax.sharding import PartitionSpec as P
 
 EPS = 1e-06
+
+
+def desk_state(in_array, axis_k):
+    return jnp.concatenate(
+        lax.all_to_all(jnp.stack(lax.axis_size("tp") * [in_array]), "tp", 0, 0), axis=axis_k
+    )
 
 
 def from_everyone(shard, axis):
@@ -52,7 +58,7 @@
     down_w = w_down[0]
     outbox = jnp.zeros((experts * capacity, share), jnp.bfloat16).at[target].set(normed[sources])
     inbox = lax.all_to_all(outbox, "ep", split_axis=0, concat_axis=0, tiled=True)
-    piece = lax.all_gather(inbox, "tp", axis=1, tiled=True)
+    piece = desk_state(inbox, 1)
     gate = jnp.dot(piece, gate_w, preferred_element_type=jnp.float32)
     up = jnp.dot(piece, up_w, preferred_element_type=jnp.float32)
     hidden = (jax.nn.silu(gate) * up).astype(jnp.bfloat16)

time: 260 us -> 230 us (0.88)
  waiting for transfers between devices: 89.3 us -> 29.9 us
  blocking collectives: 94 us -> 146 us
  between operations: 13.6 us -> 0.22 us
  starting transfers between devices: 26.6 us -> 18.4 us
  matrix products: 15.8 us -> 12 us
  local copies, waits for them, and re-layouts: 11.2 us -> 13.8 us
    all_gather x1 -> x0, waiting for transfers between devices: 59.4 us -> none  [local(): piece = lax.all_gather(inbox, 'tp', axis=1, tiled=True)]
    all_to_all x0 -> x1, blocking collectives: none -> 53.5 us  [desk_state(): lax.all_to_all(jnp.stack(lax.axis_size('tp') * [in_array]), 'tp', 0, 0)]
    all_to_all x1, starting transfers between devices: 15.5 us -> 7.29 us  [local(): lax.all_to_all(sums.astype(jnp.bfloat16), 'ep', split_axis=1, concat_axis...]
  transfers between devices with their start and end apart: 4 -> 3, of which waited for: 4 -> 3; matrix products, arithmetic and copies ran while one was open for 2% -> 2% of each run, Pallas kernels for 0% -> 0%
where the time goes in v1:
time: 230 us
  blocking collectives  146 us (63%)
  waiting for transfers between devices  29.9 us (13%)
  starting transfers between devices  18.4 us (8%)
  local copies, waits for them, and re-layouts  13.8 us (6%)
  matrix products  12 us (5%)
  other arithmetic  9.19 us (4%)
    all_to_all x1, blocking collectives, desk_state(): lax.all_to_all(jnp.stack(lax.axis_size('tp') * [in_array]), 'tp', 0, 0)  53.5 us
    all_to_all x1, blocking collectives, summed_on_arrival(): lax.all_to_all(cut_along(shard, dim, length), axis, 0, 0, tiled=True)  53.1 us
    all_to_all x1, blocking collectives, local(): lax.all_to_all(outbox, 'ep', split_axis=0, concat_axis=0, tiled=True)  39.4 us
    all_to_all x1, waiting for transfers between devices, local(): lax.all_to_all(sums.astype(jnp.bfloat16), 'ep', split_axis=1, concat_axis...  21.6 us
    all_to_all x2, starting transfers between devices, from_everyone(): return lax.all_to_all(copies, axis, split_axis=0, concat_axis=0, tiled=True)  11.1 us
    all_to_all x2, waiting for transfers between devices, from_everyone(): return lax.all_to_all(copies, axis, split_axis=0, concat_axis=0, tiled=True)  8.3 us
    dot_general x1, matrix products, local(): lax.dot_general(down_w, hidden, (((0,), (1,)), ((), ())), preferred_eleme...  7.91 us
    all_to_all x1, starting transfers between devices, local(): lax.all_to_all(sums.astype(jnp.bfloat16), 'ep', split_axis=1, concat_axis...  7.29 us
  transfers between devices with their start and end apart: 3, of which 3 were waited for; matrix products, arithmetic and copies ran while one was open for 2% of the time, Pallas kernels for 0%

profile of v1, /device:TPU:1, one launch (start us, length us, event | category | flops | bytes accessed | tf_op | source)
XLA Modules:
  0.0 229.6 jit_solution(8643207585627709610)
XLA Ops:
  0.0 0.0 copy-start
  0.0 1.1 fusion.9
  1.1 0.6 broadcast_in_dim.31
  1.7 7.6 %all-to-all-start = ((f32[16,1,256]{2,1,0:T(1,128)}), f32[16,1,256]{2,1,0:T(1,128)S(1)}, u32[]{:S(2)}, u32[]{:S(2)}) async-start(f32[16,1,256]{2,1,0:T(1,128)} %broadcast_in_dim.31), calls=%async_computation | async-start | bytes 32768 | tf_op jit(solution)/shard_map/all_to_all | solution.py:17
  9.3 0.8 copy.39
  10.1 0.1 eq.26
  10.2 0.1 reshape.129
  10.4 0.7 broadcast_multiply_fusion
  11.1 1.2 reduce-window.6
  12.3 0.2 slice_reduce_fusion
  12.5 0.1 copy.44
  12.7 0.1 mul.70
  12.8 0.1 reshape.131
  13.0 0.1 fusion.18
  13.1 0.7 convert_element_type.37
  13.8 1.9 all-to-all-done
  15.8 0.9 fusion.11
  16.7 3.1 %scatter_custom_fusion = bf16[1024,128]{1,0:T(8,128)(2,1)S(1)} fusion(s32[512]{0:T(512)S(1)} %bitcast.67, bf16[256,128]{1,0:T(8,128)(2,1)S(1)} %fusion.11, s32[1024]{0:T(1024)S(1)} %pad_clamp_fusion.1, bf16[]{:T(256)} %constant.34.clone.1), kind=kCustom, calls=%fused_computation.17 | custom fusion | bytes 262146 | tf_op jit(solution)/shard_map/scatter | solution.py:59
  19.8 39.4 %all_to_all.43 = bf16[32,32,128]{2,1,0:T(8,128)(2,1)S(1)} all-to-all(bf16[32,32,128]{2,1,0:T(8,128)(2,1)S(1)} %bitcast.61), channel_id=1, replica_groups=mesh['ep'=32,'tp'=16] {'ep'}, dimensions={0} | all-to-all | bytes 524288 | tf_op jit(solution)/shard_map/all_to_all | solution.py:60
  59.2 0.1 copy.46
  59.3 0.5 stack.5
  59.9 0.0 copy-start.4
  59.9 53.5 %all_to_all.44 = bf16[16,1024,128]{1,2,0:T(8,128)(2,1)S(1)} all-to-all(bf16[16,1024,128]{1,2,0:T(8,128)(2,1)S(1)} %stack.5), channel_id=1, replica_groups=mesh['ep'=32,'tp'=16] {'tp'}, dimensions={0} | all-to-all | bytes 8388608 | tf_op jit(solution)/shard_map/all_to_all | solution.py:11
  113.4 0.0 copy-start.1
  113.4 1.9 copy-done.1
  115.4 0.0 copy-done.4
  115.4 0.0 copy-start.5
  115.4 3.6 %fusion.3 = f32[1024,384]{1,0:T(8,128)} fusion(bf16[1024,2048]{0,1:T(8,128)(2,1)S(1)} %bitcast.59, bf16[1,2048,384]{2,1,0:T(8,128)(2,1)S(1)} %copy-done.4), kind=kOutput, calls=%fused_computation.8 | convolution fusion | flops 1610612736 | bytes 7340032 | tf_op jit(solution)/shard_map/dot_general | solution.py:62
  119.0 0.0 copy-done
  119.0 0.0 copy-done.5
  119.0 7.9 %convert_bitcast_fusion = bf16[128,16,8,128]{3,2,1,0:T(8,128)(2,1)} fusion(bf16[1,384,2048]{2,1,0:T(8,128)(2,1)S(1)} %copy-done, f32[1024,384]{1,0:T(8,128)} %fusion.3, bf16[1024,2048]{0,1:T(8,128)(2,1)} %bitcast.60, bf16[1,2048,384]{2,1,0:T(8,128)(2,1)S(1)} %copy-done.5), kind=kOutput, calls=%fused_computation.4 | convolution fusion | flops 3225681920 | bytes 13107200 | tf_op jit(solution)/shard_map/dot_general | solution.py:66
  126.9 3.3 %copy.57 = bf16[128,16,8,128]{3,2,0,1:T(8,128)(2,1)S(1)} copy(bf16[128,16,8,128]{3,2,1,0:T(8,128)(2,1)} %convert_bitcast_fusion) | data formatting | bytes 8388608 | tf_op jit(solution)/shard_map/reshape | solution.py:26
  130.1 53.1 %all_to_all.45 = bf16[16,128,1024]{1,2,0:T(8,128)(2,1)} all-to-all(bf16[16,128,1024]{1,2,0:T(8,128)(2,1)S(1)} %bitcast.57), channel_id=1, replica_groups=mesh['ep'=32,'tp'=16] {'tp'}, dimensions={0} | all-to-all | bytes 8388608 | tf_op jit(solution)/shard_map/all_to_all | solution.py:31
  183.2 0.0 copy-start.2
  183.2 0.0 copy-start.3
  183.2 3.5 %reduce_sum.66 = bf16[128,1024]{0,1:T(8,128)(2,1)} reduce(bf16[16,128,1024]{1,2,0:T(8,128)(2,1)} %all_to_all.45, bf16[]{:T(256)} %constant.34.clone.1), dimensions={0}, to_apply=%region_6.7 | reduce | flops 1966080 | bytes 4456450 | tf_op jit(solution)/shard_map/reduce_sum | solution.py:32
  186.8 7.3 %all-to-all-start.4 = ((bf16[128,32,32]{0,2,1:T(8,128)(2,1)}), bf16[128,32,32]{0,2,1:T(8,128)(2,1)S(1)}, u32[]{:S(2)}, u32[]{:S(2)}) async-start(bf16[128,32,32]{0,2,1:T(8,128)(2,1)} %bitcast.13), calls=%async_computation.4 | async-start | bytes 524288 | tf_op jit(solution)/shard_map/all_to_all | solution.py:72
  194.1 0.1 reduce_sum.62
  194.2 0.1 copy.42
  194.3 0.0 copy-done.2
  194.3 0.2 copy.43
  194.5 0.0 copy-done.3
  194.5 0.2 copy.49
  194.7 21.6 %all-to-all-done.4 = bf16[128,32,32]{0,2,1:T(8,128)(2,1)S(1)} async-done(((bf16[128,32,32]{0,2,1:T(8,128)(2,1)}), bf16[128,32,32]{0,2,1:T(8,128)(2,1)S(1)}, u32[]{:S(2)}, u32[]{:S(2)}) %all-to-all-start.4) | async-done | bytes 262176 | tf_op jit(solution)/shard_map/all_to_all | solution.py:72
  216.3 0.0 copy-start.6
  216.3 1.3 gather_fusion
  217.7 0.5 fusion.15
  218.2 0.1 multiply_reduce_fusion
  218.3 0.6 broadcast_in_dim.34
  218.9 3.5 %all-to-all-start.5 = ((f32[16,1,256]{2,1,0:T(1,128)}), f32[16,1,256]{2,1,0:T(1,128)S(1)}, u32[]{:S(2)}, u32[]{:S(2)}) async-start(f32[16,1,256]{2,1,0:T(1,128)} %broadcast_in_dim.34), calls=%async_computation.5 | async-start | bytes 32768 | tf_op jit(solution)/shard_map/all_to_all | solution.py:17
  222.4 0.0 copy-done.6
  222.4 6.4 %all-to-all-done.5 = f32[16,1,256]{2,1,0:T(1,128)S(1)} async-done(((f32[16,1,256]{2,1,0:T(1,128)}), f32[16,1,256]{2,1,0:T(1,128)S(1)}, u32[]{:S(2)}, u32[]{:S(2)}) %all-to-all-start.5) | async-done | bytes 16416 | tf_op jit(solution)/shard_map/all_to_all | solution.py:17
  228.8 0.7 multiply_convert_fusion.1
  (14 shorter events, 0.2 us)
Async XLA Ops:
  0.0 119.0 %copy-start = (bf16[1,384,2048]{2,1,0:T(8,128)(2,1)S(1)}, bf16[1,384,2048]{2,1,0:T(8,128)(2,1)}, u32[]{:S(2)}) copy-start(bf16[1,384,2048]{2,1,0:T(8,128)(2,1)} %param.12) | copy-start | bytes 4718596
  1.7 14.0 %all-to-all-start = ((f32[16,1,256]{2,1,0:T(1,128)}), f32[16,1,256]{2,1,0:T(1,128)S(1)}, u32[]{:S(2)}, u32[]{:S(2)}) async-start(f32[16,1,256]{2,1,0:T(1,128)} %broadcast_in_dim.31), calls=%async_computation | async-start | bytes 32768 | tf_op jit(solution)/shard_map/all_to_all | solution.py:17
  59.9 55.5 %copy-start.4 = (bf16[1,2048,384]{2,1,0:T(8,128)(2,1)S(1)}, bf16[1,2048,384]{2,1,0:T(8,128)(2,1)}, u32[]{:S(2)}) copy-start(bf16[1,2048,384]{2,1,0:T(8,128)(2,1)} %param.10) | copy-start | bytes 4718596
  113.4 1.9 copy-start.1
  115.4 3.6 %copy-start.5 = (bf16[1,2048,384]{2,1,0:T(8,128)(2,1)S(1)}, bf16[1,2048,384]{2,1,0:T(8,128)(2,1)}, u32[]{:S(2)}) copy-start(bf16[1,2048,384]{2,1,0:T(8,128)(2,1)} %param.11) | copy-start | bytes 4718596
  183.2 11.0 %copy-start.2 = (s32[256,2]{0,1:T(2,128)S(1)}, s32[256,2]{0,1:T(2,128)}, u32[]{:S(2)}) copy-start(s32[256,2]{0,1:T(2,128)} %param.13) | copy-start | bytes 6148
  183.2 11.3 %copy-start.3 = (f32[256,2]{0,1:T(2,128)S(1)}, f32[256,2]{0,1:T(2,128)}, u32[]{:S(2)}) copy-start(f32[256,2]{0,1:T(2,128)} %param.14) | copy-start | bytes 6148
  186.8 29.6 %all-to-all-start.4 = ((bf16[128,32,32]{0,2,1:T(8,128)(2,1)}), bf16[128,32,32]{0,2,1:T(8,128)(2,1)S(1)}, u32[]{:S(2)}, u32[]{:S(2)}) async-start(bf16[128,32,32]{0,2,1:T(8,128)(2,1)} %bitcast.13), calls=%async_computation.4 | async-start | bytes 524288 | tf_op jit(solution)/shard_map/all_to_all | solution.py:72
  216.3 6.1 %copy-start.6 = (bf16[128]{0:T(256)(128)(2,1)S(1)}, bf16[128]{0:T(256)(128)(2,1)}, u32[]{:S(2)}) copy-start(bf16[128]{0:T(256)(128)(2,1)} %param.15) | copy-start | bytes 772
  218.9 9.9 %all-to-all-start.5 = ((f32[16,1,256]{2,1,0:T(1,128)}), f32[16,1,256]{2,1,0:T(1,128)S(1)}, u32[]{:S(2)}, u32[]{:S(2)}) async-start(f32[16,1,256]{2,1,0:T(1,128)} %broadcast_in_dim.34), calls=%async_computation.5 | async-start | bytes 32768 | tf_op jit(solution)/shard_map/all_to_all | solution.py:17
